TPU v7x, 256 devices: a whole 4x4x8 slice. The times are simulated.
256 devices in a mesh: gr: 2 (over z_hi), sp: 16 (over z_lo, y), tp: 8 (over x, core).
Axes of the slice: x: 4, y: 4, z: 8 (z_hi: 2, z_lo: 4; z = z_hi * 4 + z_lo), core: 2. Of those that a mesh axis runs over, the one named last changes fastest.
Arguments:
- tokens: bfloat16 [8, 8, 2048, 4096], P('gr', 'tp', 'sp'), may hold values from -6 to 6
- ln_gain: bfloat16 [4096], replicated, may hold values from 0.099609375 to 1.8984375
- w_key: bfloat16 [4096, 256], P('sp'), may hold values from -0.09375 to 0.09375
- w_value: bfloat16 [4096, 256], P('sp'), may hold values from -0.09375 to 0.09375
- queries: bfloat16 [32, 512], P(('gr', 'sp')), may hold values from -6 to 6
- head_shift: float32 [4, 8], replicated
- key_shift: float32 [32, 16384], P(('gr', 'sp'), 'tp')
Outputs:
- kv_cache: bfloat16 [32, 16384, 128], P(('gr', 'sp'), 'tp')
- first_read: float32 [32, 512], P(('gr', 'sp'))
All inputs are finite; a program needn't handle non-finite values.
Results may differ from a plain program's by a relative error of at most 0.0064.
Values may be sent and summed in bfloat16 or wider, within the bound.
A program may use at most 64 MiB of HBM per device.

v0:
```python
import math
import jax
import jax.numpy as jnp
from jax import lax
from jax.sharding import Mesh
from jax.sharding import PartitionSpec as P

HD = 64
KVH = 4
GROUP = 8
SP = ("sp_0", "sp_1")
GR_SP = ("gr", "sp_0", "sp_1")
epsilon = 1e-05


def in_order(pieces, dim):
    pieces = jnp.moveaxis(pieces, 0, dim)
    shape = pieces.shape
    return pieces.reshape(*shape[:dim], shape[dim] * shape[dim + 1], *shape[dim + 2 :])


def stacked_from(shard, axes, sequence):
    pieces = shard[None]
    for k in sequence:
        pieces = lax.all_gather(pieces, axes[k], axis=0, tiled=True)
    carried = [lax.axis_size(axes[k]) for k in reversed(sequence)]
    pieces = pieces.reshape(*carried, *shard.shape)
    turned = sorted(range(len(sequence)), key=lambda place: sequence[len(sequence) - 1 - place])
    return pieces.transpose(*turned, *range(len(sequence), pieces.ndim)).reshape(-1, *shard.shape)


def whole_of(shard, axes, sequence, dim):
    return in_order(stacked_from(shard, axes, sequence), dim)


def side_by_side(arrays, axis, dim, along):
    widths = [math.prod(a.shape[along:]) for a in arrays]
    both = jnp.concatenate(
        [a.reshape(*a.shape[:along], w) for a, w in zip(arrays, widths)], axis=along
    )
    filled = lax.all_gather(both, axis, axis=dim, tiled=True)
    pieces = jnp.split(filled, [sum(widths[:k]) for k in range(1, len(widths))], axis=along)
    return tuple(
        (b.reshape(*filled.shape[:along], *a.shape[along:]) for a, b in zip(arrays, pieces))
    )


def add_columns(normed, segment):
    return jnp.dot(normed, segment, preferred_element_type=jnp.float32)


def local(tokens, ln_gain, w_key, w_value, queries, head_shift, key_shift):
    seq_count = tokens.shape[0]
    sub_count = tokens.shape[2]
    width = tokens.shape[3]
    flat_rows = tokens.reshape(seq_count * sub_count, width).astype(jnp.float32)
    row_mean = jnp.mean(flat_rows, axis=1, keepdims=True)
    centred = flat_rows - row_mean
    row_var = jnp.mean(centred * centred, axis=1, keepdims=True)
    normed = (centred * lax.rsqrt(row_var + epsilon) * ln_gain.astype(jnp.float32)).astype(
        jnp.bfloat16
    )
    keys = add_columns(normed, whole_of(w_key, SP, (0, 1), 0))
    values = add_columns(normed, whole_of(w_value, SP, (0, 1), 0))
    joined = jnp.concatenate(
        [
            keys.astype(jnp.bfloat16).reshape(seq_count, sub_count, KVH, HD),
            values.astype(jnp.bfloat16).reshape(seq_count, sub_count, KVH, HD),
        ],
        axis=3,
    )
    arranged = jnp.transpose(joined, (0, 2, 1, 3)).reshape(seq_count * KVH, sub_count, 2 * HD)
    cache_here = lax.all_to_all(arranged, SP, split_axis=0, concat_axis=1, tiled=True)
    own_keys = cache_here[0, :, :HD]
    own_values = cache_here[0, :, HD:]
    kv_head = lax.axis_index(SP) % KVH
    picker = (jnp.arange(KVH) == kv_head).astype(jnp.float32)
    head_row = jnp.sum(picker[:, None] * head_shift, axis=0)
    query = queries.reshape(GROUP, HD)
    logits = jnp.einsum("gd,jd->gj", query, own_keys, preferred_element_type=jnp.float32) * HD ** (
        -0.5
    )
    logits = logits + head_row[:, None] + key_shift[0][None, :]
    log_beta = jax.nn.log_sigmoid(logits)
    log_keep = log_beta - logits
    within = lax.cumsum(log_keep, axis=1, reverse=True) - log_keep
    local_weight = jnp.exp(log_beta + within).astype(jnp.bfloat16)
    section_part = jnp.dot(local_weight, own_values, preferred_element_type=jnp.float32)
    section_total = jnp.sum(log_keep, axis=1)
    all_totals, all_parts = side_by_side((section_total[None], section_part[None]), "tp", 0, 2)
    carry_all = lax.cumsum(all_totals, axis=0, reverse=True) - all_totals
    first_read = jnp.sum(jnp.exp(carry_all)[:, :, None] * all_parts, axis=0)
    return (cache_here, first_read.reshape(1, GROUP * HD))


def solution(mesh):
    split = Mesh(
        mesh.devices.reshape(mesh.shape["gr"], 4, 4, mesh.shape["tp"]), ("gr", "sp_0", "sp_1", "tp")
    )
    placed = (
        P("gr", "tp", SP, None),
        P(),
        P(SP, None),
        P(SP, None),
        P(GR_SP, None),
        P(),
        P(GR_SP, "tp"),
    )
    return jax.shard_map(
        local,
        mesh=split,
        in_specs=placed,
        out_specs=(P(GR_SP, "tp", None), P(GR_SP, None)),
        check_vma=False,
    )
```

profile of v0, /device:TPU:1, one launch (start us, length us, event | category | flops | bytes accessed | tf_op | source)
XLA Modules:
  0.0 156.6 jit_solution(1758660517415116715)
XLA Ops:
  7.2 17.0 %all-gather.1 = bf16[1024,256]{1,0:T(8,128)(2,1)} all-gather(bf16[256,256]{1,0:T(8,128)(2,1)} %param.10), channel_id=3, replica_groups=mesh['gr'=2,'sp_0'=4,'sp_1'=4,'tp'=8] {'sp_0'}, dimensions={0}, use_global_device_ids=true | all-gather | bytes 655360 | tf_op jit(solution)/shard_map/all_gather | solution.py:25
  24.3 13.4 %all-gather = bf16[1024,256]{1,0:T(8,128)(2,1)} all-gather(bf16[256,256]{1,0:T(8,128)(2,1)} %param.9), channel_id=2, replica_groups=mesh['gr'=2,'sp_0'=4,'sp_1'=4,'tp'=8] {'sp_0'}, dimensions={0}, use_global_device_ids=true | all-gather | bytes 655360 | tf_op jit(solution)/shard_map/all_gather | solution.py:25
  37.8 0.9 convert_element_type.34
  38.6 3.4 %convert_reduce_fusion = f32[4,128]{1,0:T(4,128)S(1)} fusion(bf16[4,1,128,4096]{3,2,1,0:T(8,128)(2,1)} %param.7), kind=kLoop, calls=%fused_computation.1 | loop fusion | flops 4193792 | bytes 4196352 | tf_op jit(solution)/shard_map/reduce_sum | solution.py:57
  42.1 1.2 fusion.2
  43.3 4.3 %fusion.4 = bf16[4,1,128,4096]{3,2,1,0:T(8,128)(2,1)} fusion(bf16[4,1,128,4096]{3,2,1,0:T(8,128)(2,1)S(1)} %copy-done, f32[4096]{0:T(1024)S(1)} %convert_element_type.34, f32[4,128]{1,0:T(4,128)S(1)} %add_rsqrt_fusion, f32[4,128]{1,0:T(4,128)S(1)} %broadcast_multiply_fusion), kind=kLoop, calls=%fused_computation.6 | loop fusion | flops 10485760 | bytes 8409088 | tf_op jit(solution)/shard_map/convert_element_type | solution.py:60
  47.6 12.9 %all-gather.7.cloned.1.call-done = bf16[16,256,256]{2,1,0:T(8,128)(2,1)} async-done(((bf16[4,256,256]{2,1,0:T(8,128)(2,1)}), bf16[16,256,256]{2,1,0:T(8,128)(2,1)}) %all-gather.7.cloned.1.call-update) | async-done | bytes 2097168 | tf_op jit(solution)/shard_map/all_gather | solution.py:25
  60.6 1.9 %copy.25 = bf16[4,4,256,256]{3,2,1,0:T(8,128)(2,1)S(1)} copy(bf16[4,4,256,256]{3,2,0,1:T(8,128)(2,1)} %bitcast.57) | data formatting | bytes 4194304 | tf_op jit(solution)/shard_map/transpose | solution.py:29
  62.4 0.9 copy-done.1
  63.4 1.2 convolution_convert_fusion
  64.6 0.1 copy.26
  64.8 30.9 %all-gather.5.cloned.1.call-done = bf16[16,256,256]{2,1,0:T(8,128)(2,1)} async-done(((bf16[4,256,256]{2,1,0:T(8,128)(2,1)}), bf16[16,256,256]{2,1,0:T(8,128)(2,1)}) %all-gather.5.cloned.1.call-update) | async-done | bytes 2097168 | tf_op jit(solution)/shard_map/all_gather | solution.py:25
  95.8 1.9 %copy.23 = bf16[4,4,256,256]{3,2,1,0:T(8,128)(2,1)S(1)} copy(bf16[4,4,256,256]{3,2,0,1:T(8,128)(2,1)} %bitcast.56) | data formatting | bytes 4194304 | tf_op jit(solution)/shard_map/transpose | solution.py:29
  97.7 0.9 copy-done.2
  98.6 1.2 convolution_convert_fusion.1
  99.9 0.1 copy.24
  100.1 0.3 maximum_bitcast_fusion
  100.4 1.1 copy.27
  101.5 5.8 %all-to-all-start = ((bf16[16,128,128]{2,1,0:T(8,128)(2,1)}), bf16[16,128,128]{2,1,0:T(8,128)(2,1)S(1)}, u32[]{:S(2)}, u32[]{:S(2)}) async-start(bf16[16,128,128]{2,1,0:T(8,128)(2,1)} %bitcast.10), calls=%async_computation | async-start | bytes 1048576 | tf_op jit(solution)/shard_map/all_to_all | solution.py:73
  107.4 0.1 reshape.123
  107.6 13.4 %all-to-all-done = bf16[16,128,128]{2,1,0:T(8,128)(2,1)S(1)} async-done(((bf16[16,128,128]{2,1,0:T(8,128)(2,1)}), bf16[16,128,128]{2,1,0:T(8,128)(2,1)S(1)}, u32[]{:S(2)}, u32[]{:S(2)}) %all-to-all-start) | async-done | bytes 524320 | tf_op jit(solution)/shard_map/all_to_all | solution.py:73
  121.0 0.2 fusion.7
  121.3 0.2 fusion.18
  121.5 9.9 %reduce-window.6 = f32[8,16,128]{2,1,0:T(8,128)S(1)} reduce-window(f32[8,16,128]{2,1,0:T(8,128)S(1)} %copy.28, f32[]{:T(128)} %constant.30.clone.1), window={size=1x1x128 pad=0_0x0_0x0_127}, to_apply=%region_4.5 | reduce-window | flops 2080768 | bytes 131076 | tf_op jit(solution)/shard_map/reduce-window
  131.4 0.1 slice_reduce_fusion
  131.5 0.2 reduce-window.9
  131.8 0.3 convolution_bitcast_fusion
  132.3 15.7 %all_gather.19 = f32[8,8,65]{2,1,0:T(8,128)S(1)} all-gather(f32[1,8,65]{2,1,0:T(8,128)S(1)} %pad_maximum_fusion), channel_id=1, replica_groups=mesh['gr'=2,'sp_0'=4,'sp_1'=4,'tp'=8] {'tp'}, dimensions={0}, use_global_device_ids=true | all-gather | bytes 18720 | tf_op jit(solution)/shard_map/all_gather | solution.py:41
  148.0 0.1 copy.31
  148.2 0.1 fusion.14
  148.3 0.7 reshape.126
  149.0 0.8 copy.36
  (28 shorter events, 0.8 us)
Async XLA Ops:
  7.2 53.4 %all-gather.7.cloned.1.call-start = ((), (), s32[]{:S(2)}) async-start(), calls=%async_computation.2 | async-start | bytes 2621440 | tf_op jit(solution)/shard_map/all_gather | solution.py:25
  24.3 71.5 %all-gather.5.cloned.1.call-start = ((), (), s32[]{:S(2)}) async-start(), calls=%async_computation.1 | async-start | bytes 2621440 | tf_op jit(solution)/shard_map/all_gather | solution.py:25
  37.8 4.3 %copy-start = (bf16[4,1,128,4096]{3,2,1,0:T(8,128)(2,1)S(1)}, bf16[4,1,128,4096]{3,2,1,0:T(8,128)(2,1)}, u32[]{:S(2)}) copy-start(bf16[4,1,128,4096]{3,2,1,0:T(8,128)(2,1)} %param.7) | copy-start | bytes 12582916
  60.6 2.8 %copy-start.1 = (bf16[4,1,128,4096]{3,2,1,0:T(8,128)(2,1)S(1)}, bf16[4,1,128,4096]{3,2,1,0:T(8,128)(2,1)}, u32[]{:S(2)}) copy-start(bf16[4,1,128,4096]{3,2,1,0:T(8,128)(2,1)} %fusion.4) | copy-start | bytes 12582916
  95.8 2.8 %copy-start.2 = (bf16[4,1,128,4096]{3,2,1,0:T(8,128)(2,1)S(1)}, bf16[4,1,128,4096]{3,2,1,0:T(8,128)(2,1)}, u32[]{:S(2)}) copy-start(bf16[4,1,128,4096]{3,2,1,0:T(8,128)(2,1)} %fusion.4) | copy-start | bytes 12582916
  98.6 8.8 %copy-start.3 = (bf16[1,512]{1,0:T(2,128)(2,1)S(1)}, bf16[1,512]{1,0:T(2,128)(2,1)}, u32[]{:S(2)}) copy-start(bf16[1,512]{1,0:T(2,128)(2,1)} %param.11) | copy-start | bytes 3076
  98.6 8.9 %copy-start.4 = (f32[4,8]{1,0:T(4,128)S(1)}, f32[4,8]{1,0:T(4,128)}, u32[]{:S(2)}) copy-start(f32[4,8]{1,0:T(4,128)} %param.12) | copy-start | bytes 388
  98.6 22.4 %copy-start.5 = (f32[1,2048]{1,0:T(1,128)S(1)}, f32[1,2048]{1,0:T(1,128)}, u32[]{:S(2)}) copy-start(f32[1,2048]{1,0:T(1,128)} %param.13) | copy-start | bytes 24580
  101.5 19.5 %all-to-all-start = ((bf16[16,128,128]{2,1,0:T(8,128)(2,1)}), bf16[16,128,128]{2,1,0:T(8,128)(2,1)S(1)}, u32[]{:S(2)}, u32[]{:S(2)}) async-start(bf16[16,128,128]{2,1,0:T(8,128)(2,1)} %bitcast.10), calls=%async_computation | async-start | bytes 1048576 | tf_op jit(solution)/shard_map/all_to_all | solution.py:73
Sparse Core Ops, SparseCore 0:
  24.4 36.1 all-gather.6
  62.4 33.3 all-gather.4
where the time goes:
time: 157 us
  waiting for transfers between devices  57.3 us (36%)
  blocking collectives  46.2 us (29%)
  other arithmetic  20.9 us (13%)
  between operations  14.2 us (9%)
  local copies, waits for them, and re-layouts  9.08 us (6%)
  starting transfers between devices  5.9 us (4%)
  matrix products  3.04 us (2%)
    all_gather x2, waiting for transfers between devices, stacked_from(): pieces = lax.all_gather(pieces, axes[k], axis=0, tiled=True)  43.9 us
    all_gather x2, blocking collectives, stacked_from(): pieces = lax.all_gather(pieces, axes[k], axis=0, tiled=True)  30.5 us
    all_gather x1, blocking collectives, side_by_side(): filled = lax.all_gather(both, axis, axis=dim, tiled=True)  15.7 us
    all_to_all x1, waiting for transfers between devices, local(): lax.all_to_all(arranged, SP, split_axis=0, concat_axis=1, tiled=True)  13.4 us
    another operation x2, other arithmetic  10.1 us
    all_to_all x1, starting transfers between devices, local(): lax.all_to_all(arranged, SP, split_axis=0, concat_axis=1, tiled=True)  5.82 us
    convert_element_type x1, other arithmetic, local(): (centred * lax.rsqrt(row_var + epsilon) * ln_gain.astype(jnp.float32)).as...  4.3 us
    transpose x2, local copies, waits for them, and re-layouts, stacked_from(): pieces.transpose(*turned, *range(len(sequence), pieces.ndim))  3.76 us
  transfers between devices with their start and end apart: 3, of which 3 were waited for; matrix products, arithmetic and copies ran while one was open for 9% of the time, Pallas kernels for 0%

commit v1 on v0

--- a/solution.py
+++ b/solution.py
@@ -70,7 +70,9 @@
         axis=3,
     )
     arranged = jnp.transpose(joined, (0, 2, 1, 3)).reshape(seq_count * KVH, sub_count, 2 * HD)
-    cache_here = lax.all_to_all(arranged, SP, split_axis=0, concat_axis=1, tiled=True)
+    cache_here = jnp.concatenate(
+        lax.all_to_all(jnp.stack(jnp.split(arranged, lax.axis_size(SP), axis=0)), SP, 0, 0), axis=1
+    )
     own_keys = cache_here[0, :, :HD]
     own_values = cache_here[0, :, HD:]
     kv_head = lax.axis_index(SP) % KVH

time: 157 us -> 166 us (1.057)
  local copies, waits for them, and re-layouts: 9.08 us -> 18.2 us
    unnamed x14 -> x29, local copies, waits for them, and re-layouts: 2.79 us -> 12.1 us
  transfers between devices with their start and end apart: 3 -> 3, of which waited for: 3 -> 3; matrix products, arithmetic and copies ran while one was open for 9% -> 8% of each run, Pallas kernels for 0% -> 0%
where the time goes in v1:
time: 166 us
  waiting for transfers between devices  57.4 us (35%)
  blocking collectives  46.2 us (28%)
  other arithmetic  20.8 us (13%)
  local copies, waits for them, and re-layouts  18.2 us (11%)
  between operations  14.2 us (9%)
  starting transfers between devices  5.9 us (4%)
  matrix products  3.04 us (2%)
    all_gather x2, waiting for transfers between devices, stacked_from(): pieces = lax.all_gather(pieces, axes[k], axis=0, tiled=True)  43.9 us
    all_gather x2, blocking collectives, stacked_from(): pieces = lax.all_gather(pieces, axes[k], axis=0, tiled=True)  30.4 us
    all_gather x1, blocking collectives, side_by_side(): filled = lax.all_gather(both, axis, axis=dim, tiled=True)  15.7 us
    all_to_all x1, waiting for transfers between devices, local(): lax.all_to_all(jnp.stack(jnp.split(arranged, lax.axis_size(SP), axis=0)),...  13.4 us
    unnamed x29, local copies, waits for them, and re-layouts  12.1 us
    another operation x2, other arithmetic  10.1 us
    all_to_all x1, starting transfers between devices, local(): lax.all_to_all(jnp.stack(jnp.split(arranged, lax.axis_size(SP), axis=0)),...  5.82 us
    convert_element_type x1, other arithmetic, local(): (centred * lax.rsqrt(row_var + epsilon) * ln_gain.astype(jnp.float32)).as...  4.3 us
  transfers between devices with their start and end apart: 3, of which 3 were waited for; matrix products, arithmetic and copies ran while one was open for 8% of the time, Pallas kernels for 0%

profile of v1, /device:TPU:1, one launch (start us, length us, event | category | flops | bytes accessed | tf_op | source)
XLA Modules:
  0.0 165.8 jit_solution(400030235128817751)
XLA Ops:
  7.2 17.0 %all-gather = bf16[1024,256]{1,0:T(8,128)(2,1)} all-gather(bf16[256,256]{1,0:T(8,128)(2,1)} %param.9), channel_id=2, replica_groups=mesh['gr'=2,'sp_0'=4,'sp_1'=4,'tp'=8] {'sp_0'}, dimensions={0}, use_global_device_ids=true | all-gather | bytes 655360 | tf_op jit(solution)/shard_map/all_gather | solution.py:25
  24.3 13.4 %all-gather.1 = bf16[1024,256]{1,0:T(8,128)(2,1)} all-gather(bf16[256,256]{1,0:T(8,128)(2,1)} %param.10), channel_id=3, replica_groups=mesh['gr'=2,'sp_0'=4,'sp_1'=4,'tp'=8] {'sp_0'}, dimensions={0}, use_global_device_ids=true | all-gather | bytes 655360 | tf_op jit(solution)/shard_map/all_gather | solution.py:25
  37.8 0.9 convert_element_type.34
  38.6 3.4 %convert_reduce_fusion = f32[4,128]{1,0:T(4,128)S(1)} fusion(bf16[4,1,128,4096]{3,2,1,0:T(8,128)(2,1)} %param.7), kind=kLoop, calls=%fused_computation.1 | loop fusion | flops 4193792 | bytes 4196352 | tf_op jit(solution)/shard_map/reduce_sum | solution.py:57
  42.1 1.2 fusion.2
  43.3 4.3 %fusion.4 = bf16[4,1,128,4096]{3,2,1,0:T(8,128)(2,1)} fusion(bf16[4,1,128,4096]{3,2,1,0:T(8,128)(2,1)S(1)} %copy-done, f32[4096]{0:T(1024)S(1)} %convert_element_type.34, f32[4,128]{1,0:T(4,128)S(1)} %add_rsqrt_fusion, f32[4,128]{1,0:T(4,128)S(1)} %broadcast_multiply_fusion), kind=kLoop, calls=%fused_computation.6 | loop fusion | flops 10485760 | bytes 8409088 | tf_op jit(solution)/shard_map/convert_element_type | solution.py:60
  47.6 13.0 %all-gather.5.cloned.1.call-done = bf16[16,256,256]{2,1,0:T(8,128)(2,1)} async-done(((bf16[4,256,256]{2,1,0:T(8,128)(2,1)}), bf16[16,256,256]{2,1,0:T(8,128)(2,1)}) %all-gather.5.cloned.1.call-update) | async-done | bytes 2097168 | tf_op jit(solution)/shard_map/all_gather | solution.py:25
  60.6 1.9 %copy.38 = bf16[4,4,256,256]{3,2,1,0:T(8,128)(2,1)S(1)} copy(bf16[4,4,256,256]{3,2,0,1:T(8,128)(2,1)} %bitcast.137) | data formatting | bytes 4194304 | tf_op jit(solution)/shard_map/transpose | solution.py:29
  62.5 0.9 copy-done.1
  63.4 1.2 convolution_convert_fusion.1
  64.9 30.9 %all-gather.7.cloned.1.call-done = bf16[16,256,256]{2,1,0:T(8,128)(2,1)} async-done(((bf16[4,256,256]{2,1,0:T(8,128)(2,1)}), bf16[16,256,256]{2,1,0:T(8,128)(2,1)}) %all-gather.7.cloned.1.call-update) | async-done | bytes 2097168 | tf_op jit(solution)/shard_map/all_gather | solution.py:25
  95.8 1.9 %copy.40 = bf16[4,4,256,256]{3,2,1,0:T(8,128)(2,1)S(1)} copy(bf16[4,4,256,256]{3,2,0,1:T(8,128)(2,1)} %bitcast.136) | data formatting | bytes 4194304 | tf_op jit(solution)/shard_map/transpose | solution.py:29
  97.7 0.9 copy-done.2
  98.6 1.2 convolution_convert_fusion
  100.9 0.6 constant_dynamic-update-slice_fusion.15
  101.5 0.6 constant_dynamic-update-slice_fusion.14
  102.1 0.6 constant_dynamic-update-slice_fusion.13
  102.7 0.6 constant_dynamic-update-slice_fusion.12
  103.3 0.6 constant_dynamic-update-slice_fusion.11
  103.9 0.6 constant_dynamic-update-slice_fusion.10
  104.6 0.6 constant_dynamic-update-slice_fusion.9
  105.2 0.6 constant_dynamic-update-slice_fusion.8
  105.8 0.6 constant_dynamic-update-slice_fusion.7
  106.4 0.6 constant_dynamic-update-slice_fusion.6
  107.0 0.6 constant_dynamic-update-slice_fusion.5
  107.6 0.6 constant_dynamic-update-slice_fusion.4
  110.7 5.8 %all-to-all-start = ((bf16[16,1,128,128]{3,2,1,0:T(8,128)(2,1)}), bf16[16,1,128,128]{3,2,1,0:T(8,128)(2,1)S(1)}, u32[]{:S(2)}, u32[]{:S(2)}) async-start(bf16[16,1,128,128]{3,2,1,0:T(8,128)(2,1)} %constant_dynamic-update-slice_fusion), calls=%async_computation | async-start | bytes 1048576 | tf_op jit(solution)/shard_map/all_to_all | solution.py:74
  116.8 13.4 %all-to-all-done = bf16[16,1,128,128]{3,2,1,0:T(8,128)(2,1)S(1)} async-done(((bf16[16,1,128,128]{3,2,1,0:T(8,128)(2,1)}), bf16[16,1,128,128]{3,2,1,0:T(8,128)(2,1)S(1)}, u32[]{:S(2)}, u32[]{:S(2)}) %all-to-all-start) | async-done | bytes 524320 | tf_op jit(solution)/shard_map/all_to_all | solution.py:74
  130.7 9.9 %reduce-window.6 = f32[8,16,128]{2,1,0:T(8,128)S(1)} reduce-window(f32[8,16,128]{2,1,0:T(8,128)S(1)} %copy.43, f32[]{:T(128)} %constant.30.clone.1), window={size=1x1x128 pad=0_0x0_0x0_127}, to_apply=%region_4.5 | reduce-window | flops 2080768 | bytes 131076 | tf_op jit(solution)/shard_map/reduce-window
  141.5 15.7 %all_gather.19 = f32[8,8,65]{2,1,0:T(8,128)S(1)} all-gather(f32[1,8,65]{2,1,0:T(8,128)S(1)} %pad_maximum_fusion), channel_id=1, replica_groups=mesh['gr'=2,'sp_0'=4,'sp_1'=4,'tp'=8] {'tp'}, dimensions={0}, use_global_device_ids=true | all-gather | bytes 18720 | tf_op jit(solution)/shard_map/all_gather | solution.py:41
  157.5 0.7 reshape.127
  158.2 0.8 copy.66
  (44 shorter events, 5.5 us)
Async XLA Ops:
  7.2 53.4 %all-gather.5.cloned.1.call-start = ((), (), s32[]{:S(2)}) async-start(), calls=%async_computation.1 | async-start | bytes 2621440 | tf_op jit(solution)/shard_map/all_gather | solution.py:25
  24.3 71.5 %all-gather.7.cloned.1.call-start = ((), (), s32[]{:S(2)}) async-start(), calls=%async_computation.2 | async-start | bytes 2621440 | tf_op jit(solution)/shard_map/all_gather | solution.py:25
  37.7 4.3 %copy-start = (bf16[4,1,128,4096]{3,2,1,0:T(8,128)(2,1)S(1)}, bf16[4,1,128,4096]{3,2,1,0:T(8,128)(2,1)}, u32[]{:S(2)}) copy-start(bf16[4,1,128,4096]{3,2,1,0:T(8,128)(2,1)} %param.7) | copy-start | bytes 12582916
  60.6 2.8 %copy-start.1 = (bf16[4,1,128,4096]{3,2,1,0:T(8,128)(2,1)S(1)}, bf16[4,1,128,4096]{3,2,1,0:T(8,128)(2,1)}, u32[]{:S(2)}) copy-start(bf16[4,1,128,4096]{3,2,1,0:T(8,128)(2,1)} %fusion.4) | copy-start | bytes 12582916
  95.8 2.8 %copy-start.2 = (bf16[4,1,128,4096]{3,2,1,0:T(8,128)(2,1)S(1)}, bf16[4,1,128,4096]{3,2,1,0:T(8,128)(2,1)}, u32[]{:S(2)}) copy-start(bf16[4,1,128,4096]{3,2,1,0:T(8,128)(2,1)} %fusion.4) | copy-start | bytes 12582916
  99.9 16.7 %copy-start.3 = (bf16[1,512]{1,0:T(2,128)(2,1)S(1)}, bf16[1,512]{1,0:T(2,128)(2,1)}, u32[]{:S(2)}) copy-start(bf16[1,512]{1,0:T(2,128)(2,1)} %param.11) | copy-start | bytes 3076
  99.9 16.8 %copy-start.4 = (f32[4,8]{1,0:T(4,128)S(1)}, f32[4,8]{1,0:T(4,128)}, u32[]{:S(2)}) copy-start(f32[4,8]{1,0:T(4,128)} %param.12) | copy-start | bytes 388
  99.9 30.3 %copy-start.5 = (f32[1,2048]{1,0:T(1,128)S(1)}, f32[1,2048]{1,0:T(1,128)}, u32[]{:S(2)}) copy-start(f32[1,2048]{1,0:T(1,128)} %param.13) | copy-start | bytes 24580
  110.7 19.5 %all-to-all-start = ((bf16[16,1,128,128]{3,2,1,0:T(8,128)(2,1)}), bf16[16,1,128,128]{3,2,1,0:T(8,128)(2,1)S(1)}, u32[]{:S(2)}, u32[]{:S(2)}) async-start(bf16[16,1,128,128]{3,2,1,0:T(8,128)(2,1)} %constant_dynamic-update-slice_fusion), calls=%async_computation | async-start | bytes 1048576 | tf_op jit(solution)/shard_map/all_to_all | solution.py:74
Sparse Core Ops, SparseCore 0:
  24.4 36.1 all-gather.4
  62.4 33.3 all-gather.6
